TPU v7x, 32 devices: a whole 2x2x4 slice. The times are simulated.
32 devices in a mesh: rep: 2 (over x), fs: 4 (over z), tp: 4 (over y, core).
Axes of the slice: x: 2, y: 2, z: 4, core: 2. Of those that a mesh axis runs over, the one named last changes fastest.
Arguments:
- tokens: bfloat16 [4096, 2048], P(('rep', 'fs', 'tp')), may hold values from -6 to 6
- norm_gain: float32 [2048], replicated, may hold values from 0.1 to 1.9
- gate_weight: float32 [2048, 5632], P('fs', 'tp'), may hold values from -0.125 to 0.125
- gate_scale: float32 [5632], P('tp'), may hold values from 0.5 to 2
- up_weight: float32 [2048, 5632], P('fs', 'tp'), may hold values from -0.125 to 0.125
- up_scale: float32 [5632], P('tp'), may hold values from 0.5 to 2
- down_weight: float32 [5632, 2048], P('tp', 'fs'), may hold values from -0.078125 to 0.078125
- down_scale: float32 [2048], P('fs'), may hold values from 0.5 to 2
Outputs:
- mixed: bfloat16 [4096, 2048], P(('rep', 'fs', 'tp'))
All inputs are finite; a program needn't handle non-finite values.
Results may differ from a plain program's by a relative error of at most 0.014.
Values may be sent and summed in bfloat16 or wider, within the bound.
A program may use at most 64 MiB of HBM per device.

v0:
```python
import jax
import jax.numpy as jnp
from jax import lax
from jax.sharding import PartitionSpec as P


def shards(
    tokens, norm_gain, gate_weight, gate_scale, up_weight, up_scale, down_weight, down_scale
):
    n_rep = lax.axis_size("rep")
    rep = lax.axis_index("rep")
    width = gate_weight.shape[1] // n_rep
    start = rep * width

    def part(array, axis):
        return lax.dynamic_slice_in_dim(array, start, width, axis)

    flat = tokens.astype(jnp.float32)
    mean_square = jnp.mean(flat * flat, axis=-1, keepdims=True)
    inverse = lax.rsqrt(mean_square + 1e-06)
    normed = (flat * inverse * norm_gain).astype(jnp.bfloat16)
    group = lax.all_gather(normed, ("rep", "tp"), axis=0, tiled=True)
    gate_low = part(gate_weight, 1).astype(jnp.bfloat16)
    up_low = part(up_weight, 1).astype(jnp.bfloat16)
    down_low = part(down_weight, 0).astype(jnp.bfloat16)
    gate = jnp.dot(
        group,
        lax.all_gather(gate_low, "fs", axis=0, tiled=True),
        preferred_element_type=jnp.float32,
    )
    up = jnp.dot(
        group, lax.all_gather(up_low, "fs", axis=0, tiled=True), preferred_element_type=jnp.float32
    )
    down_full = lax.all_gather(down_low, "fs", axis=1, tiled=True)
    gate = gate * part(gate_scale, 0)
    up = up * part(up_scale, 0)
    hidden = (jax.nn.silu(gate) * up).astype(jnp.bfloat16)
    scales = lax.all_gather(down_scale, "fs", axis=0, tiled=True)
    total = lax.psum_scatter(
        jnp.dot(hidden, down_full, preferred_element_type=jnp.float32).astype(jnp.bfloat16),
        ("rep", "tp"),
        scatter_dimension=0,
        tiled=True,
    ).astype(jnp.float32)
    return (total * scales).astype(jnp.bfloat16)


def solution(mesh):
    in_specs = (
        P(("rep", "fs", "tp"), None),
        P(),
        P("fs", "tp"),
        P("tp"),
        P("fs", "tp"),
        P("tp"),
        P("tp", "fs"),
        P("fs"),
    )
    out_specs = P(("rep", "fs", "tp"), None)
    return jax.shard_map(shards, mesh=mesh, in_specs=in_specs, out_specs=out_specs, check_vma=False)
```

profile of v0, /device:TPU:0, one launch (start us, length us, event | category | flops | bytes accessed | tf_op | source)
XLA Modules:
  0.0 308.1 jit_solution(6207909742359432319)
XLA Ops:
  6.6 1.8 copy-done
  8.4 1.2 dynamic-slice_convert_fusion.1
  9.6 0.0 all-gather.8.cloned.1.call-update
  9.6 0.0 all-gather.6.cloned.1.call-start
  9.7 1.2 fusion
  10.9 1.0 fusion.2
  11.9 0.0 all-gather.6.cloned.1.call-update
  11.9 0.0 all-gather.10.cloned.1.call-start
  12.0 2.7 dynamic-slice_convert_fusion
  14.8 0.0 all-gather.12.cloned.1.call-start
  14.8 2.3 dynamic-slice_convert_fusion.2
  17.2 0.0 reduce-scatter.2.cloned.1.call-start
  17.2 0.1 dynamic_slice.16
  17.3 0.1 dynamic_slice.18
  17.4 58.6 %all-gather.8.cloned.1.call-done = bf16[2048,704]{1,0:T(8,128)(2,1)} async-done(((bf16[512,704]{1,0:T(8,128)(2,1)}), bf16[2048,704]{1,0:T(8,128)(2,1)}) %all-gather.8.cloned.1.call-update) | async-done | bytes 2883600 | tf_op jit(solution)/shard_map/all_gather | solution.py:28
  75.9 37.1 %all-gather.6.cloned.1.call-done = bf16[1024,2048]{1,0:T(8,128)(2,1)} async-done(((bf16[128,2048]{1,0:T(8,128)(2,1)}), bf16[1024,2048]{1,0:T(8,128)(2,1)}) %all-gather.6.cloned.1.call-update) | async-done | bytes 4194320 | tf_op jit(solution)/shard_map/all_gather | solution.py:22
  113.1 7.9 %fusion.4 = f32[1024,704]{0,1:T(8,128)} fusion(bf16[1024,2048]{1,0:T(8,128)(2,1)} %all-gather.6.cloned.1.call-done, bf16[2048,704]{1,0:T(8,128)(2,1)} %all-gather.8.cloned.1.call-done), kind=kOutput, calls=%fused_computation.13 | convolution fusion | flops 2952790016 | bytes 9961472 | tf_op jit(solution)/shard_map/dot_general | solution.py:26
  121.0 57.1 %all-gather.10.cloned.1.call-done = bf16[2048,704]{1,0:T(8,128)(2,1)} async-done(((bf16[512,704]{1,0:T(8,128)(2,1)}), bf16[2048,704]{1,0:T(8,128)(2,1)}) %all-gather.10.cloned.1.call-update) | async-done | bytes 2883600 | tf_op jit(solution)/shard_map/all_gather | solution.py:32
  178.1 59.2 %all-gather.12.cloned.1.call-done = bf16[704,2048]{1,0:T(8,128)(2,1)} async-done(((bf16[704,512]{1,0:T(8,128)(2,1)}), bf16[704,2048]{1,0:T(8,128)(2,1)}) %all-gather.12.cloned.1.call-update) | async-done | bytes 2883600 | tf_op jit(solution)/shard_map/all_gather | solution.py:34
  237.3 12.3 %convolution_convert_fusion = bf16[1024,2048]{1,0:T(8,128)(2,1)} fusion(bf16[704,2048]{1,0:T(8,128)(2,1)} %all-gather.12.cloned.1.call-done, f32[1024,704]{0,1:T(8,128)} %fusion.4, bf16[1024,2048]{1,0:T(8,128)(2,1)} %all-gather.6.cloned.1.call-done, bf16[2048,704]{1,0:T(8,128)(2,1)} %all-gather.10.cloned.1.call-done, f32[704]{0:T(1024)S(1)} %dynamic_slice.18, ...), kind=kOutput, calls=%fused_computation | convolution fusion | flops 5913444352 | bytes 17044992 | tf_op jit(solution)/shard_map/dot_general | solution.py:40
  249.7 0.7 copy-done.3
  250.3 11.9 %all-gather = f32[4,1,512]{2,1,0:T(1,128)S(1)} all-gather(f32[1,1,512]{2,1,0:T(1,128)S(1)} %bitcast.8), channel_id=1, replica_groups=mesh['rep'=2,'fs'=4,'tp'=4] {'fs'}, dimensions={0}, use_global_device_ids=true | all-gather | bytes 10240 | tf_op jit(solution)/shard_map/all_gather | solution.py:38
  262.3 37.4 %reduce-scatter.2.cloned.1.call-done = bf16[128,2048]{1,0:T(8,128)(2,1)} async-done(((bf16[1024,2048]{1,0:T(8,128)(2,1)}), bf16[128,2048]{1,0:T(8,128)(2,1)}) %reduce-scatter.2.cloned.1.call-update) | async-done | bytes 524304 | tf_op jit(solution)/shard_map/reduce_scatter | solution.py:39
  299.7 1.9 multiply_convert_fusion.1
  (15 shorter events, 0.1 us)
Async XLA Ops:
  6.5 1.8 copy-start
  6.5 4.4 %copy-start.1 = (bf16[128,2048]{1,0:T(8,128)(2,1)S(1)}, bf16[128,2048]{1,0:T(8,128)(2,1)}, u32[]{:S(2)}) copy-start(bf16[128,2048]{1,0:T(8,128)(2,1)} %param.8) | copy-start | bytes 1572868
  6.5 4.4 %copy-start.2 = (f32[2048]{0:T(1024)S(1)}, f32[2048]{0:T(1024)}, u32[]{:S(2)}) copy-start(f32[2048]{0:T(1024)} %param.9) | copy-start | bytes 24580
  6.5 69.4 %all-gather.8.cloned.1.call-start = ((), (), s32[]{:S(2)}) async-start(), calls=%async_computation.2 | async-start | bytes 3932160 | tf_op jit(solution)/shard_map/all_gather | solution.py:28
  9.6 103.5 %all-gather.6.cloned.1.call-start = ((), (), s32[]{:S(2)}) async-start(), calls=%async_computation.1 | async-start | bytes 4718592 | tf_op jit(solution)/shard_map/all_gather | solution.py:22
  10.9 6.3 %copy-start.4 = (f32[1408]{0:T(1024)S(1)}, f32[1408]{0:T(1024)}, u32[]{:S(2)}) copy-start(f32[1408]{0:T(1024)} %param.11) | copy-start | bytes 16900
  10.9 6.4 %copy-start.5 = (f32[1408]{0:T(1024)S(1)}, f32[1408]{0:T(1024)}, u32[]{:S(2)}) copy-start(f32[1408]{0:T(1024)} %param.13) | copy-start | bytes 16900
  11.9 166.2 %all-gather.10.cloned.1.call-start = ((), (), s32[]{:S(2)}) async-start(), calls=%async_computation.3 | async-start | bytes 3932160 | tf_op jit(solution)/shard_map/all_gather | solution.py:32
  14.8 222.6 %all-gather.12.cloned.1.call-start = ((), (), s32[]{:S(2)}) async-start(), calls=%async_computation.4 | async-start | bytes 3604480 | tf_op jit(solution)/shard_map/all_gather | solution.py:34
  17.2 282.5 %reduce-scatter.2.cloned.1.call-start = ((), (), s32[]{:S(2)}) async-start(), calls=%async_computation.5 | async-start | bytes 4718592 | tf_op jit(solution)/shard_map/reduce_scatter | solution.py:39
  249.7 0.7 copy-start.3
Sparse Core Ops, SparseCore 0:
  9.7 66.1 all-gather.7
  77.8 35.2 all-gather.5
  114.7 63.4 all-gather.9
  179.6 57.7 all-gather.11
  249.8 49.8 reduce-scatter.1
where the time goes:
time: 308 us
  waiting for transfers between devices  250 us (81%)
  matrix products  20.2 us (7%)
  between operations  13.2 us (4%)
  blocking collectives  11.9 us (4%)
  local copies, waits for them, and re-layouts  8.92 us (3%)
  other arithmetic  4.16 us (1%)
    all_gather x1, waiting for transfers between devices, shards(): down_full = lax.all_gather(down_low, 'fs', axis=1, tiled=True)  59.2 us
    all_gather x1, waiting for transfers between devices, shards(): lax.all_gather(gate_low, 'fs', axis=0, tiled=True)  58.6 us
    all_gather x1, waiting for transfers between devices, shards(): lax.all_gather(up_low, 'fs', axis=0, tiled=True)  57.1 us
    reduce_scatter x1, waiting for transfers between devices, shards(): lax.psum_scatter(jnp.dot(hidden, down_full, preferred_element_type=jnp.fl...  37.4 us
    all_gather x1, waiting for transfers between devices, shards(): group = lax.all_gather(normed, ('rep', 'tp'), axis=0, tiled=True)  37.1 us
    dot_general x1, matrix products, shards(): jnp.dot(hidden, down_full, preferred_element_type=jnp.float32)  12.3 us
    all_gather x1, blocking collectives, shards(): scales = lax.all_gather(down_scale, 'fs', axis=0, tiled=True)  11.9 us
    dot_general x1, matrix products, shards(): jnp.dot(group, lax.all_gather(gate_low, 'fs', axis=0, tiled=True), prefer...  7.9 us
  transfers between devices with their start and end apart: 5, of which 5 were waited for; matrix products, arithmetic and copies ran while one was open for 5% of the time, Pallas kernels for 0%

commit v1 on v0

--- a/solution.py
+++ b/solution.py
@@ -31,7 +31,16 @@
     up = jnp.dot(
         group, lax.all_gather(up_low, "fs", axis=0, tiled=True), preferred_element_type=jnp.float32
     )
-    down_full = lax.all_gather(down_low, "fs", axis=1, tiled=True)
+    ways = lax.axis_size("fs")
+    up_2 = [(d, (d + 1) % ways) for d in range(ways)]
+    down = [(d, (d - 1) % ways) for d in range(ways)]
+    earlier, later = ([down_low], [down_low])
+    for _ in range(ways // 2):
+        earlier.append(lax.ppermute(earlier[-1], "fs", up_2))
+    for _ in range((ways - 1) // 2):
+        later.append(lax.ppermute(later[-1], "fs", down))
+    line = jnp.concatenate([*earlier[::-1], *later[1:]], axis=1)
+    down_full = jnp.roll(line, (lax.axis_index("fs") - ways // 2) * down_low.shape[1], axis=1)
     gate = gate * part(gate_scale, 0)
     up = up * part(up_scale, 0)
     hidden = (jax.nn.silu(gate) * up).astype(jnp.bfloat16)

time: 308 us -> 287 us (0.932)
  waiting for transfers between devices: 250 us -> 189 us
  starting transfers between devices: 0.17 us -> 20.6 us
  local copies, waits for them, and re-layouts: 8.92 us -> 26.2 us
    ppermute x0 -> x3, waiting for transfers between devices: none -> 74.9 us  [the longest x2 66.5 us: shards(): earlier.append(lax.ppermute(earlier[-1], 'fs', up_2))]
    all_gather x1 -> x0, waiting for transfers between devices: 59.2 us -> none  [shards(): down_full = lax.all_gather(down_low, 'fs', axis=1, tiled=True)]
    all_gather x1, waiting for transfers between devices: 58.6 us -> 0.01 us  [shards(): lax.all_gather(gate_low, 'fs', axis=0, tiled=True)]
    ppermute x0 -> x3, starting transfers between devices: none -> 20.5 us  [the longest x2 18.1 us: shards(): earlier.append(lax.ppermute(earlier[-1], 'fs', up_2))]
    all_gather x1, waiting for transfers between devices: 37.1 us -> 20 us  [shards(): group = lax.all_gather(normed, ('rep', 'tp'), axis=0, tiled=True)]
    unnamed x12 -> x15, local copies, waits for them, and re-layouts: 2.48 us -> 17.7 us
  transfers between devices with their start and end apart: 5 -> 7, of which waited for: 5 -> 6; matrix products, arithmetic and copies ran while one was open for 5% -> 12% of each run, Pallas kernels for 0% -> 0%
where the time goes in v1:
time: 287 us
  waiting for transfers between devices  189 us (66%)
  local copies, waits for them, and re-layouts  26.2 us (9%)
  starting transfers between devices  20.6 us (7%)
  matrix products  20.2 us (7%)
  between operations  13.2 us (5%)
  blocking collectives  11.9 us (4%)
  other arithmetic  5.2 us (2%)
    ppermute x2, waiting for transfers between devices, shards(): earlier.append(lax.ppermute(earlier[-1], 'fs', up_2))  66.5 us
    all_gather x1, waiting for transfers between devices, shards(): lax.all_gather(up_low, 'fs', axis=0, tiled=True)  57.2 us
    reduce_scatter x1, waiting for transfers between devices, shards(): lax.psum_scatter(jnp.dot(hidden, down_full, preferred_element_type=jnp.fl...  37.4 us
    all_gather x1, waiting for transfers between devices, shards(): group = lax.all_gather(normed, ('rep', 'tp'), axis=0, tiled=True)  20 us
    ppermute x2, starting transfers between devices, shards(): earlier.append(lax.ppermute(earlier[-1], 'fs', up_2))  18.1 us
    unnamed x15, local copies, waits for them, and re-layouts  17.7 us
    dot_general x1, matrix products, shards(): jnp.dot(hidden, down_full, preferred_element_type=jnp.float32)  12.3 us
    all_gather x1, blocking collectives, shards(): scales = lax.all_gather(down_scale, 'fs', axis=0, tiled=True)  11.9 us
  transfers between devices with their start and end apart: 7, of which 6 were waited for; matrix products, arithmetic and copies ran while one was open for 12% of the time, Pallas kernels for 0%

profile of v1, /device:TPU:0, one launch (start us, length us, event | category | flops | bytes accessed | tf_op | source)
XLA Modules:
  0.0 286.8 jit_solution(6783128986484985410)
XLA Ops:
  10.9 2.0 fusion.3
  13.0 2.7 dynamic-slice_convert_fusion
  15.8 2.3 dynamic-slice_convert_fusion.2
  18.2 3.1 %collective-permute-start = (bf16[704,512]{1,0:T(8,128)(2,1)}, bf16[704,512]{1,0:T(8,128)(2,1)}, u32[]{:S(2)}, u32[]{:S(2)}) collective-permute-start(bf16[704,512]{1,0:T(8,128)(2,1)} %dynamic-slice_convert_fusion.2), channel_id=1, source_target_pairs={{0,4},{4,8},{8,12},{12,0},{1,5},{5,9},{9,13},{13,1},{2,6},{6,10},{... | collective-permute-start | bytes 2162696 | tf_op jit(solution)/shard_map/ppermute | solution.py:39
  21.2 33.9 %collective-permute-done = bf16[704,512]{1,0:T(8,128)(2,1)} collective-permute-done((bf16[704,512]{1,0:T(8,128)(2,1)}, bf16[704,512]{1,0:T(8,128)(2,1)}, u32[]{:S(2)}, u32[]{:S(2)}) %collective-permute-start) | collective-permute-done | bytes 720928 | tf_op jit(solution)/shard_map/ppermute | solution.py:39
  55.1 15.1 %collective-permute-start.1 = (bf16[704,512]{1,0:T(8,128)(2,1)}, bf16[704,512]{1,0:T(8,128)(2,1)}, u32[]{:S(2)}, u32[]{:S(2)}) collective-permute-start(bf16[704,512]{1,0:T(8,128)(2,1)} %collective-permute-done), channel_id=1, source_target_pairs={{0,4},{4,8},{8,12},{12,0},{1,5},{5,9},{9,13},{13,1},{2,6},{6,10},{... | collective-permute-start | bytes 2162696 | tf_op jit(solution)/shard_map/ppermute | solution.py:39
  70.2 2.4 collective-permute-start.2
  72.7 32.6 %collective-permute-done.1 = bf16[704,512]{1,0:T(8,128)(2,1)} collective-permute-done((bf16[704,512]{1,0:T(8,128)(2,1)}, bf16[704,512]{1,0:T(8,128)(2,1)}, u32[]{:S(2)}, u32[]{:S(2)}) %collective-permute-start.1) | collective-permute-done | bytes 720928 | tf_op jit(solution)/shard_map/ppermute | solution.py:39
  105.3 2.1 constant_dynamic-update-slice_fusion.7
  107.4 2.1 constant_dynamic-update-slice_fusion.6
  109.4 2.4 constant_dynamic-update-slice_fusion.5
  111.8 8.4 %collective-permute-done.2 = bf16[704,512]{1,0:T(8,128)(2,1)} collective-permute-done((bf16[704,512]{1,0:T(8,128)(2,1)}, bf16[704,512]{1,0:T(8,128)(2,1)}, u32[]{:S(2)}, u32[]{:S(2)}) %collective-permute-start.2) | collective-permute-done | bytes 720928 | tf_op jit(solution)/shard_map/ppermute | solution.py:41
  120.2 2.2 constant_dynamic-update-slice_fusion.4
  122.3 2.2 constant_dynamic-update-slice_fusion.3
  124.5 2.1 constant_dynamic-update-slice_fusion.2
  126.6 2.4 constant_dynamic-update-slice_fusion.1
  128.9 2.1 constant_dynamic-update-slice_fusion
  131.0 20.0 %all-gather.5.cloned.1.call-done = bf16[1024,2048]{1,0:T(8,128)(2,1)} async-done(((bf16[128,2048]{1,0:T(8,128)(2,1)}), bf16[1024,2048]{1,0:T(8,128)(2,1)}) %all-gather.5.cloned.1.call-update) | async-done | bytes 4194320 | tf_op jit(solution)/shard_map/all_gather | solution.py:22
  151.0 7.9 %fusion.6 = f32[1024,704]{0,1:T(8,128)} fusion(bf16[1024,2048]{1,0:T(8,128)(2,1)} %all-gather.5.cloned.1.call-done, bf16[2048,704]{1,0:T(8,128)(2,1)} %all-gather.7.cloned.1.call-done), kind=kOutput, calls=%fused_computation.23 | convolution fusion | flops 2952790016 | bytes 9961472 | tf_op jit(solution)/shard_map/dot_general | solution.py:26
  158.9 57.2 %all-gather.9.cloned.1.call-done = bf16[2048,704]{1,0:T(8,128)(2,1)} async-done(((bf16[512,704]{1,0:T(8,128)(2,1)}), bf16[2048,704]{1,0:T(8,128)(2,1)}) %all-gather.9.cloned.1.call-update) | async-done | bytes 2883600 | tf_op jit(solution)/shard_map/all_gather | solution.py:32
  216.0 12.3 %convolution_convert_fusion = bf16[1024,2048]{1,0:T(8,128)(2,1)} fusion(bf16[704,4096]{1,0:T(8,128)(2,1)} %constant_dynamic-update-slice_fusion, s32[]{:T(128)S(6)} %select_n.22, f32[1024,704]{0,1:T(8,128)} %fusion.6, bf16[1024,2048]{1,0:T(8,128)(2,1)} %all-gather.5.cloned.1.call-done, bf16[2048,704]{1,0:T(8,128)(2,1)} %all-gather.9.cloned.1.call-done, ...), kind=kOutput, calls=%fused_computation | convolution fusion | flops 5913444352 | bytes 17307140 | tf_op jit(solution)/shard_map/dot_general | solution.py:49
  229.0 11.9 %all-gather = f32[4,1,512]{2,1,0:T(1,128)S(1)} all-gather(f32[1,1,512]{2,1,0:T(1,128)S(1)} %bitcast.7), channel_id=1, replica_groups=mesh['rep'=2,'fs'=4,'tp'=4] {'fs'}, dimensions={0}, use_global_device_ids=true | all-gather | bytes 10240 | tf_op jit(solution)/shard_map/all_gather | solution.py:47
  240.9 37.4 %reduce-scatter.2.cloned.1.call-done = bf16[128,2048]{1,0:T(8,128)(2,1)} async-done(((bf16[1024,2048]{1,0:T(8,128)(2,1)}), bf16[128,2048]{1,0:T(8,128)(2,1)}) %reduce-scatter.2.cloned.1.call-update) | async-done | bytes 524304 | tf_op jit(solution)/shard_map/reduce_scatter | solution.py:48
  278.3 1.9 multiply_convert_fusion.1
  (22 shorter events, 5.3 us)
Async XLA Ops:
  6.5 1.8 copy-start
  6.5 66.0 %copy-start.2 = (f32[1408]{0:T(1024)S(1)}, f32[1408]{0:T(1024)}, u32[]{:S(2)}) copy-start(f32[1408]{0:T(1024)} %param.11) | copy-start | bytes 16900
  6.5 66.1 %copy-start.3 = (f32[1408]{0:T(1024)S(1)}, f32[1408]{0:T(1024)}, u32[]{:S(2)}) copy-start(f32[1408]{0:T(1024)} %param.13) | copy-start | bytes 16900
  6.5 124.4 %all-gather.7.cloned.1.call-start = ((), (), s32[]{:S(2)}) async-start(), calls=%async_computation.2 | async-start | bytes 3932160 | tf_op jit(solution)/shard_map/all_gather | solution.py:28
  9.6 141.4 %all-gather.5.cloned.1.call-start = ((), (), s32[]{:S(2)}) async-start(), calls=%async_computation.1 | async-start | bytes 4718592 | tf_op jit(solution)/shard_map/all_gather | solution.py:22
  13.0 203.1 %all-gather.9.cloned.1.call-start = ((), (), s32[]{:S(2)}) async-start(), calls=%async_computation.3 | async-start | bytes 3932160 | tf_op jit(solution)/shard_map/all_gather | solution.py:32
  15.8 262.6 %reduce-scatter.2.cloned.1.call-start = ((), (), s32[]{:S(2)}) async-start(), calls=%async_computation.4 | async-start | bytes 4718592 | tf_op jit(solution)/shard_map/reduce_scatter | solution.py:48
  18.2 37.0 %collective-permute-start = (bf16[704,512]{1,0:T(8,128)(2,1)}, bf16[704,512]{1,0:T(8,128)(2,1)}, u32[]{:S(2)}, u32[]{:S(2)}) collective-permute-start(bf16[704,512]{1,0:T(8,128)(2,1)} %dynamic-slice_convert_fusion.2), channel_id=1, source_target_pairs={{0,4},{4,8},{8,12},{12,0},{1,5},{5,9},{9,13},{13,1},{2,6},{6,10},{... | collective-permute-start | bytes 2162696 | tf_op jit(solution)/shard_map/ppermute | solution.py:39
  55.1 50.2 %collective-permute-start.1 = (bf16[704,512]{1,0:T(8,128)(2,1)}, bf16[704,512]{1,0:T(8,128)(2,1)}, u32[]{:S(2)}, u32[]{:S(2)}) collective-permute-start(bf16[704,512]{1,0:T(8,128)(2,1)} %collective-permute-done), channel_id=1, source_target_pairs={{0,4},{4,8},{8,12},{12,0},{1,5},{5,9},{9,13},{13,1},{2,6},{6,10},{... | collective-permute-start | bytes 2162696 | tf_op jit(solution)/shard_map/ppermute | solution.py:39
  70.2 50.0 %collective-permute-start.2 = (bf16[704,512]{1,0:T(8,128)(2,1)}, bf16[704,512]{1,0:T(8,128)(2,1)}, u32[]{:S(2)}, u32[]{:S(2)}) collective-permute-start(bf16[704,512]{1,0:T(8,128)(2,1)} %dynamic-slice_convert_fusion.2), channel_id=1, source_target_pairs={{0,12},{4,0},{8,4},{12,8},{1,13},{5,1},{9,5},{13,9},{2,14},{6,2},{... | collective-permute-start | bytes 2162696 | tf_op jit(solution)/shard_map/ppermute | solution.py:41
  228.3 0.7 copy-start.1
Sparse Core Ops, SparseCore 0:
  9.7 104.5 all-gather.6
  116.2 34.6 all-gather.4
  152.5 63.4 all-gather.8
  228.5 49.8 reduce-scatter.1
